TPU v7x, 512 devices: a whole 4x4x16 slice. The times are simulated.
512 devices in a mesh: rep: 16 (over z), fs: 4 (over y), tp: 8 (over x, core).
Axes of the slice: x: 4, y: 4, z: 16, core: 2. Of those that a mesh axis runs over, the one named last changes fastest.
Arguments:
- inputs: bfloat16 [8192, 2048], P('rep', 'fs'), may hold values from -6 to 6
- w_gate: bfloat16 [2048, 3072], P('fs', 'tp'), may hold values from -0.125 to 0.125
- w_up: bfloat16 [2048, 3072], P('fs', 'tp'), may hold values from -0.125 to 0.125
- conv_taps: bfloat16 [3, 3072], P(None, 'tp'), may hold values from -3.5 to 3.5
- w_down: bfloat16 [3072, 2048], P('tp', 'fs'), may hold values from -0.109375 to 0.109375
- out_grad: bfloat16 [8192, 2048], P('rep', 'fs'), may hold values from -6 to 6
Outputs:
- in_grad: bfloat16 [8192, 2048], P(('rep', 'tp'), 'fs')
- grad_gate: float32 [2048, 3072], P('fs', 'tp')
- grad_up: float32 [2048, 3072], P('fs', 'tp')
- grad_down: float32 [3072, 2048], P('tp', 'fs')
- grad_taps: float32 [3, 3072], P(None, 'tp')
- rows_gate: float32 [2048], P('fs')
- rows_up: float32 [2048], P('fs')
- rows_down: float32 [3072], P('tp')
All inputs are finite; a program needn't handle non-finite values.
Results may differ from a plain program's by a relative error of at most 0.025.
Values may be sent and summed in bfloat16 or wider, within the bound.
No kernel may reach another device: no remote copies, remote signals or barrier semaphores. Data moves between devices by JAX's collectives and lax.ppermute only.
A program may use at most 64 MiB of HBM per device.

v0:
```python
import jax
import jax.numpy as jnp
from jax import lax
from jax.sharding import PartitionSpec as P

KW = 3


def shift_down(values, lag_rows):
    if lag_rows == 0:
        return values
    padding = jnp.zeros_like(values[:lag_rows])
    return jnp.concatenate([padding, values[:-lag_rows]], axis=0)


def shift_up(values, lag_rows):
    if lag_rows == 0:
        return values
    padding = jnp.zeros_like(values[:lag_rows])
    return jnp.concatenate([values[lag_rows:], padding], axis=0)


def contract(left, right, left_dim, right_dim):
    return lax.dot_general(
        left, right, (((left_dim,), (right_dim,)), ((), ())), preferred_element_type=jnp.float32
    )


def row_norms(grad_gate, grad_up, grad_down):
    gate_rows = jnp.sum(grad_gate * grad_gate, axis=1)
    up_rows = jnp.sum(grad_up * grad_up, axis=1)
    down_rows = jnp.sum(grad_down * grad_down, axis=1)
    gate_rows, up_rows = lax.psum((gate_rows, up_rows), "tp")
    down_rows = lax.psum(down_rows, "fs")
    return (gate_rows, up_rows, down_rows)


def shards(inputs, w_gate, w_up, conv_taps, w_down, out_grad):
    tap_weights = conv_taps.astype(jnp.float32)
    gate_part = jnp.dot(inputs, w_gate, preferred_element_type=jnp.float32)
    up_part = jnp.dot(inputs, w_up, preferred_element_type=jnp.float32)
    act_part = contract(out_grad, w_down, 1, 1)
    gate_sum, up_sum, act_sum = (
        lax.psum(gate_part.astype(jnp.bfloat16), "fs").astype(jnp.float32),
        lax.psum(up_part.astype(jnp.bfloat16), "fs").astype(jnp.float32),
        lax.psum(act_part.astype(jnp.bfloat16), "fs").astype(jnp.float32),
    )
    gate_pre = gate_sum.astype(jnp.bfloat16)
    up_val = up_sum.astype(jnp.bfloat16)
    act_grad = act_sum.astype(jnp.bfloat16)
    gate_float = gate_pre.astype(jnp.float32)
    up_float = up_val.astype(jnp.float32)
    act_float = act_grad.astype(jnp.float32)
    shifted = [shift_down(gate_float, KW - 1 - tap_index) for tap_index in range(KW)]
    pre_act = tap_weights[0] * shifted[0]
    for tap_index in range(1, KW):
        pre_act = pre_act + tap_weights[tap_index] * shifted[tap_index]
    sigmoid_pre = jax.nn.sigmoid(pre_act)
    hidden = (pre_act * sigmoid_pre * up_float).astype(jnp.bfloat16)
    up_grad = (act_float * pre_act * sigmoid_pre).astype(jnp.bfloat16)
    pre_grad = act_float * up_float * sigmoid_pre * (1.0 + pre_act * (1.0 - sigmoid_pre))
    gate_acc = tap_weights[0] * shift_up(pre_grad, KW - 1)
    for tap_index in range(1, KW):
        gate_acc = gate_acc + tap_weights[tap_index] * shift_up(pre_grad, KW - 1 - tap_index)
    gate_grad = gate_acc.astype(jnp.bfloat16)
    gate_rows = gate_grad
    up_rows = up_grad
    in_grad = lax.psum_scatter(
        (contract(gate_rows, w_gate, 1, 1) + contract(up_rows, w_up, 1, 1)).astype(jnp.bfloat16),
        "tp",
        scatter_dimension=0,
        tiled=True,
    )
    grad_gate = contract(inputs, gate_grad, 0, 0)
    grad_up = contract(inputs, up_grad, 0, 0)
    grad_down = contract(hidden, out_grad, 0, 0)
    grad_taps = jnp.stack(
        [jnp.sum(shifted[tap_index] * pre_grad, axis=0) for tap_index in range(KW)]
    )
    grad_gate, grad_up, grad_down, grad_taps = (
        lax.psum(grad_gate.astype(jnp.bfloat16), "rep").astype(jnp.float32),
        lax.psum(grad_up.astype(jnp.bfloat16), "rep").astype(jnp.float32),
        lax.psum(grad_down.astype(jnp.bfloat16), "rep").astype(jnp.float32),
        lax.psum(grad_taps.astype(jnp.bfloat16), "rep").astype(jnp.float32),
    )
    gate_rows, up_rows, down_rows = row_norms(grad_gate, grad_up, grad_down)
    weight_grads = (grad_gate, grad_up, grad_down, grad_taps, gate_rows, up_rows, down_rows)
    grad_gate, grad_up, grad_down, grad_taps, gate_rows, up_rows, down_rows = weight_grads
    return (in_grad, grad_gate, grad_up, grad_down, grad_taps, gate_rows, up_rows, down_rows)


def solution(mesh):
    return jax.shard_map(
        shards,
        mesh=mesh,
        in_specs=(
            P("rep", "fs"),
            P("fs", "tp"),
            P("fs", "tp"),
            P(None, "tp"),
            P("tp", "fs"),
            P("rep", "fs"),
        ),
        out_specs=(
            P(("rep", "tp"), "fs"),
            P("fs", "tp"),
            P("fs", "tp"),
            P("tp", "fs"),
            P(None, "tp"),
            P("fs"),
            P("fs"),
            P("tp"),
        ),
        check_vma=False,
    )
```

profile of v0, /device:TPU:1, one launch (start us, length us, event | category | flops | bytes accessed | tf_op | source)
XLA Modules:
  0.0 273.1 jit_solution(11521428086460877337)
XLA Ops:
  7.2 1.0 copy-done
  8.2 2.2 convolution_convert_fusion.3
  10.4 1.2 convolution_convert_fusion.4
  11.6 1.2 convolution_convert_fusion.5
  12.9 0.6 copy-done.11
  13.5 65.6 %all-reduce.12.cloned.1.call-done = (bf16[512,384]{1,0:T(8,128)(2,1)}, bf16[512,384]{1,0:T(8,128)(2,1)}, bf16[512,384]{1,0:T(8,128)(2,1)}) async-done(((bf16[512,384]{1,0:T(8,128)(2,1)}, bf16[512,384]{1,0:T(8,128)(2,1)}, bf16[512,384]{1,0:T(8,128)(2,1)}), (bf16[512,384]{1,0:T(8,128)(2,1)}, bf16[512,384]{1,0:T(8,128)(2,1)}, bf16[512,384]{1,0:T(8,128)(2,1)})) %all-reduce.12.cloned.1.call-update) | async-done | bytes 1179664 | tf_op jit(solution)/shard_map/psum | solution.py:44
  79.1 1.1 slice.32
  80.4 0.9 copy-done.2
  81.4 0.8 multiply_reduce_fusion.5
  82.3 1.2 convolution_convert_fusion
  83.9 1.1 fusion.1
  85.0 1.1 fusion.2
  86.2 0.9 copy-done.3
  87.2 0.5 fusion.11
  87.6 1.3 fusion
  89.0 24.9 %psum.76 = bf16[3,384]{1,0:T(4,128)(2,1)S(1)} all-reduce(bf16[3,384]{1,0:T(4,128)(2,1)S(1)} %pad_maximum_fusion), channel_id=1, replica_groups=mesh['rep'=16,'fs'=4,'tp'=8] {'rep'}, use_global_device_ids=true, to_apply=%region_10.0 | all-reduce | flops 1152 | bytes 4608 | tf_op jit(solution)/shard_map/psum | solution.py:84
  113.8 0.6 convert_element_type.86
  114.4 104.8 %all-reduce.10.cloned.1.call-done = (bf16[512,384]{0,1:T(8,128)(2,1)}, bf16[512,384]{0,1:T(8,128)(2,1)}, bf16[384,512]{1,0:T(8,128)(2,1)}) async-done(((bf16[512,384]{0,1:T(8,128)(2,1)}, bf16[512,384]{0,1:T(8,128)(2,1)}, bf16[384,512]{1,0:T(8,128)(2,1)}), (bf16[512,384]{0,1:T(8,128)(2,1)}, bf16[512,384]{0,1:T(8,128)(2,1)}, bf16[384,512]{1,0:T(8,128)(2,1)})) %all-reduce.10.cloned.1.call-update) | async-done | bytes 1179664 | tf_op jit(solution)/shard_map/psum | solution.py:81
  219.2 2.1 copy.14
  221.3 1.1 copy.15
  222.4 1.0 multiply_reduce_fusion
  223.4 9.2 %psum.79 = f32[384]{0:T(512)} all-reduce(f32[384]{0:T(512)S(1)} %get-tuple-element.30), channel_id=1, replica_groups=mesh['rep'=16,'fs'=4,'tp'=8] {'fs'}, use_global_device_ids=true, to_apply=%region_16.0 | all-reduce | flops 384 | bytes 3072 | tf_op jit(solution)/shard_map/psum | solution.py:34
  232.8 24.5 %all-reduce.4 = (f32[512]{0:T(512)}, f32[512]{0:T(512)}) all-reduce(f32[512]{0:T(512)S(1)} %multiply_reduce_fusion.2, f32[512]{0:T(512)S(1)} %multiply_reduce_fusion.1), channel_id=1, replica_groups=mesh['rep'=16,'fs'=4,'tp'=8] {'tp'}, use_global_device_ids=true, to_apply=%region_12.0 | all-reduce | flops 1024 | bytes 8192 | tf_op jit(solution)/shard_map/psum | solution.py:33
  257.3 9.2 %reduce-scatter.2.cloned.1.call-done = bf16[64,512]{1,0:T(8,128)(2,1)} async-done(((bf16[512,512]{1,0:T(8,128)(2,1)}), bf16[64,512]{1,0:T(8,128)(2,1)}) %reduce-scatter.2.cloned.1.call-update) | async-done | bytes 65552 | tf_op jit(solution)/shard_map/reduce_scatter | solution.py:68
  (38 shorter events, 1.2 us)
Async XLA Ops:
  7.2 1.0 copy-start
  7.2 3.2 %copy-start.4 = (bf16[512,384]{1,0:T(8,128)(2,1)S(1)}, bf16[512,384]{1,0:T(8,128)(2,1)}, u32[]{:S(2)}) copy-start(bf16[512,384]{1,0:T(8,128)(2,1)} %param.8) | copy-start | bytes 1179652
  7.2 72.0 %all-reduce.12.cloned.1.call-start = ((), (), s32[]{:S(2)}) async-start(), calls=%async_computation.3 | async-start | bytes 2359296 | tf_op jit(solution)/shard_map/psum | solution.py:44
  10.4 1.2 copy-start.7
  10.4 1.2 copy-start.9
  12.8 0.7 copy-start.11
  12.8 206.4 %all-reduce.10.cloned.1.call-start = ((), (), s32[]{:S(2)}) async-start(), calls=%async_computation.2 | async-start | bytes 2359296 | tf_op jit(solution)/shard_map/psum | solution.py:81
  79.1 1.1 copy-start.1
  80.3 1.0 copy-start.2
  80.3 1.1 copy-start.8
  86.2 1.0 copy-start.3
  86.2 180.3 %reduce-scatter.2.cloned.1.call-start = ((), (), s32[]{:S(2)}) async-start(), calls=%async_computation.1 | async-start | bytes 589824 | tf_op jit(solution)/shard_map/reduce_scatter | solution.py:68
  219.2 2.1 copy-start.6
  221.3 1.1 copy-start.10
  223.4 9.4 %copy-start.5 = (bf16[512,384]{0,1:T(8,128)(2,1)S(1)}, bf16[512,384]{0,1:T(8,128)(2,1)}, u32[]{:S(2)}) copy-start(bf16[512,384]{0,1:T(8,128)(2,1)} %get-tuple-element.24) | copy-start | bytes 1179652
Sparse Core Ops, SparseCore 0:
  12.9 66.1 all-reduce.11
  86.3 132.8 all-reduce.9
  222.6 43.8 reduce-scatter.1
where the time goes:
time: 274 us; the launch traced here: 273 us
  waiting for transfers between devices  180 us (66%)
  blocking collectives  58.6 us (21%)
  between operations  13.9 us (5%)
  matrix products  9.79 us (4%)
  local copies, waits for them, and re-layouts  8.06 us (3%)
  other arithmetic  2.95 us (1%)
    psum x1, waiting for transfers between devices, shards(): lax.psum(grad_gate.astype(jnp.bfloat16), 'rep').astype(jnp.float32)  105 us
    psum x1, waiting for transfers between devices, shards(): lax.psum(gate_part.astype(jnp.bfloat16), 'fs').astype(jnp.float32)  65.6 us
    psum x1, blocking collectives, shards(): lax.psum(grad_taps.astype(jnp.bfloat16), 'rep').astype(jnp.float32)  24.9 us
    psum x1, blocking collectives, row_norms(): gate_rows, up_rows = lax.psum((gate_rows, up_rows), 'tp')  24.5 us
    psum x1, blocking collectives, row_norms(): down_rows = lax.psum(down_rows, 'fs')  9.23 us
    reduce_scatter x1, waiting for transfers between devices, shards(): lax.psum_scatter((contract(gate_rows, w_gate, 1, 1) + contract(up_rows, w...  9.19 us
    unnamed x26, local copies, waits for them, and re-layouts  6.73 us
    dot_general x6, matrix products, contract(): lax.dot_general(left, right, (((left_dim,), (right_dim,)), ((), ())), pre...  6.42 us
  transfers between devices with their start and end apart: 3, of which 3 were waited for; matrix products, arithmetic and copies ran while one was open for 2% of the time, Pallas kernels for 0%

commit v1 on v0

v1 whole, which is shorter than its diff:
```python
import jax
import jax.numpy as jnp
from jax import lax
from jax.sharding import PartitionSpec as P

KW = 3
CHUNK = 64


def shift_down(values, lag_rows):
    if lag_rows == 0:
        return values
    padding = jnp.zeros_like(values[:lag_rows])
    return jnp.concatenate([padding, values[:-lag_rows]], axis=0)


def shift_up(values, lag_rows):
    if lag_rows == 0:
        return values
    padding = jnp.zeros_like(values[:lag_rows])
    return jnp.concatenate([values[lag_rows:], padding], axis=0)


def contract(left, right, left_dim, right_dim):
    return lax.dot_general(
        left, right, (((left_dim,), (right_dim,)), ((), ())), preferred_element_type=jnp.float32
    )


def pieces(array, rows):
    return [array[start : start + rows] for start in range(0, array.shape[0], rows)]


def summed(arrays, axis, extra):
    parts = [pieces(array, CHUNK * 384 // array.shape[1]) for array in arrays]
    flat = [piece for group in parts for piece in group]
    tails = [extra[:1], extra[1:]]
    sums = lax.psum(tuple(flat + tails), axis)
    out = []
    at = 0
    for group in parts:
        out.append(jnp.concatenate(sums[at : at + len(group)], axis=0))
        at += len(group)
    return out, jnp.concatenate(sums[at:])


def split_float(values):
    high = values.astype(jnp.bfloat16)
    low = (values - high.astype(jnp.float32)).astype(jnp.bfloat16)
    return high, low


def shards(inputs, w_gate, w_up, conv_taps, w_down, out_grad):
    tap_weights = conv_taps.astype(jnp.float32)
    gate_part = jnp.dot(inputs, w_gate, preferred_element_type=jnp.float32)
    up_part = jnp.dot(inputs, w_up, preferred_element_type=jnp.float32)
    act_part = contract(out_grad, w_down, 1, 1)
    act_part = act_part.astype(jnp.bfloat16)
    (gate_pre, up_val, act_body), act_last = summed(
        [gate_part.astype(jnp.bfloat16), up_part.astype(jnp.bfloat16), act_part[:-CHUNK]],
        "fs",
        act_part[-CHUNK:].reshape(-1),
    )
    act_grad = jnp.concatenate([act_body, act_last.reshape(CHUNK, -1)], axis=0)
    gate_float = gate_pre.astype(jnp.float32)
    up_float = up_val.astype(jnp.float32)
    act_float = act_grad.astype(jnp.float32)
    shifted = [shift_down(gate_float, KW - 1 - tap_index) for tap_index in range(KW)]
    pre_act = tap_weights[0] * shifted[0]
    for tap_index in range(1, KW):
        pre_act = pre_act + tap_weights[tap_index] * shifted[tap_index]
    sigmoid_pre = jax.nn.sigmoid(pre_act)
    hidden = (pre_act * sigmoid_pre * up_float).astype(jnp.bfloat16)
    up_grad = (act_float * pre_act * sigmoid_pre).astype(jnp.bfloat16)
    pre_grad = act_float * up_float * sigmoid_pre * (1.0 + pre_act * (1.0 - sigmoid_pre))
    gate_acc = tap_weights[0] * shift_up(pre_grad, KW - 1)
    for tap_index in range(1, KW):
        gate_acc = gate_acc + tap_weights[tap_index] * shift_up(pre_grad, KW - 1 - tap_index)
    gate_grad = gate_acc.astype(jnp.bfloat16)
    grad_taps = jnp.stack(
        [jnp.sum(shifted[tap_index] * pre_grad, axis=0) for tap_index in range(KW)]
    )
    grad_gate = contract(inputs, gate_grad, 0, 0).astype(jnp.bfloat16)
    grad_up = contract(inputs, up_grad, 0, 0).astype(jnp.bfloat16)
    grad_down = contract(hidden, out_grad, 0, 0).astype(jnp.bfloat16)
    in_part = (contract(gate_grad, w_gate, 1, 1) + contract(up_grad, w_up, 1, 1)).astype(jnp.bfloat16)
    (grad_gate, grad_up, grad_down), grad_taps = summed(
        [grad_gate, grad_up, grad_down], "rep", grad_taps.astype(jnp.bfloat16).reshape(-1)
    )
    grad_gate = grad_gate.astype(jnp.float32)
    grad_up = grad_up.astype(jnp.float32)
    grad_down = grad_down.astype(jnp.float32)
    grad_taps = grad_taps.astype(jnp.float32).reshape(KW, -1)
    gate_rows = jnp.sum(grad_gate * grad_gate, axis=1)
    up_rows = jnp.sum(grad_up * grad_up, axis=1)
    down_rows = jnp.sum(grad_down * grad_down, axis=1)
    n_tp = lax.axis_size("tp")
    n_fs = lax.axis_size("fs")
    rows = jnp.stack([*split_float(gate_rows), *split_float(up_rows)])
    sent = jnp.concatenate(
        [
            in_part.reshape(n_tp, -1, in_part.shape[1]),
            jnp.broadcast_to(rows, (n_tp, *rows.shape)),
        ],
        axis=1,
    )
    got = lax.all_to_all(sent, "tp", 0, 0).astype(jnp.float32).sum(axis=0)
    n_rows = in_part.shape[0] // n_tp
    in_grad = got[:n_rows].astype(jnp.bfloat16)
    gate_rows = got[n_rows] + got[n_rows + 1]
    up_rows = got[n_rows + 2] + got[n_rows + 3]
    down_rows = lax.all_to_all(
        jnp.broadcast_to(down_rows, (n_fs, *down_rows.shape)), "fs", 0, 0
    ).sum(axis=0)
    return (in_grad, grad_gate, grad_up, grad_down, grad_taps, gate_rows, up_rows, down_rows)


def solution(mesh):
    return jax.shard_map(
        shards,
        mesh=mesh,
        in_specs=(
            P("rep", "fs"),
            P("fs", "tp"),
            P("fs", "tp"),
            P(None, "tp"),
            P("tp", "fs"),
            P("rep", "fs"),
        ),
        out_specs=(
            P(("rep", "tp"), "fs"),
            P("fs", "tp"),
            P("fs", "tp"),
            P("tp", "fs"),
            P(None, "tp"),
            P("fs"),
            P("fs"),
            P("tp"),
        ),
        check_vma=False,
    )
```

time: 274 us -> 160 us (0.58)
  waiting for transfers between devices: 180 us -> 6.68 us
  blocking collectives: 58.6 us -> 98.7 us
  starting transfers between devices: 0.12 us -> 26.9 us
  between operations: 13.9 us -> 1.22 us
  local copies, waits for them, and re-layouts: 8.06 us -> 15.2 us
  matrix products: 9.79 us -> 4.73 us
  other arithmetic: 2.95 us -> 6.01 us
    psum x2 -> x0, waiting for transfers between devices: 170 us -> none  [the longest x1 105 us: shards(): lax.psum(grad_gate.astype(jnp.bfloat16), 'rep').astype(jnp.float32)]
    psum x3 -> x2, blocking collectives: 58.6 us -> 98.7 us  [summed(): sums = lax.psum(tuple(flat + tails), axis)]
    all_to_all x0 -> x2, starting transfers between devices: none -> 26.9 us  [the longest x1 23.3 us: shards(): got = lax.all_to_all(sent, 'tp', 0, 0).astype(jnp.float32).sum(axis=0)]
    reduce_scatter x1 -> x0, waiting for transfers between devices: 9.19 us -> none  [shards(): lax.psum_scatter((contract(gate_rows, w_gate, 1, 1) + contract(up_rows, w...]
    all_to_all x0 -> x2, waiting for transfers between devices: none -> 6.68 us  [the longest x1 6.03 us: shards(): got = lax.all_to_all(sent, 'tp', 0, 0).astype(jnp.float32).sum(axis=0)]
    unnamed x26 -> x72, local copies, waits for them, and re-layouts: 6.73 us -> 10.5 us
  transfers between devices with their start and end apart: 3 -> 2, of which waited for: 3 -> 2; matrix products, arithmetic and copies ran while one was open for 2% -> 4% of each run, Pallas kernels for 0% -> 0%
where the time goes in v1:
time: 160 us; the launch traced here: 159 us
  blocking collectives  98.7 us (62%)
  starting transfers between devices  26.9 us (17%)
  local copies, waits for them, and re-layouts  15.2 us (10%)
  waiting for transfers between devices  6.68 us (4%)
  other arithmetic  6.01 us (4%)
  matrix products  4.73 us (3%)
    psum x2, blocking collectives, summed(): sums = lax.psum(tuple(flat + tails), axis)  98.7 us
    all_to_all x1, starting transfers between devices, shards(): got = lax.all_to_all(sent, 'tp', 0, 0).astype(jnp.float32).sum(axis=0)  23.3 us
    unnamed x72, local copies, waits for them, and re-layouts  10.5 us
    all_to_all x1, waiting for transfers between devices, shards(): got = lax.all_to_all(sent, 'tp', 0, 0).astype(jnp.float32).sum(axis=0)  6.03 us
    dot_general x6, matrix products, contract(): lax.dot_general(left, right, (((left_dim,), (right_dim,)), ((), ())), pre...  3.85 us
    all_to_all x1, starting transfers between devices, shards(): lax.all_to_all(jnp.broadcast_to(down_rows, (n_fs, *down_rows.shape)), 'fs...  3.61 us
  transfers between devices with their start and end apart: 2, of which 2 were waited for; matrix products, arithmetic and copies ran while one was open for 4% of the time, Pallas kernels for 0%

profile of v1, /device:TPU:1, one launch (start us, length us, event | category | flops | bytes accessed | tf_op | source)
XLA Modules:
  0.0 159.5 jit_solution(5617017776293712679)
XLA Ops:
  0.7 1.7 %convolution_convert_fusion.5 = bf16[512,384]{1,0:T(8,128)(2,1)S(1)} fusion(bf16[512,512]{1,0:T(8,128)(2,1)} %param.11, bf16[384,512]{1,0:T(8,128)(2,1)} %param.10), kind=kOutput, calls=%fused_computation.7 | convolution fusion | flops 201523200 | bytes 1310720 | tf_op jit(solution)/shard_map/dot_general | solution.py:25
  4.6 29.7 %all-reduce.8 = (bf16[64,384]{1,0:T(8,128)(2,1)S(1)}, bf16[64,384]{1,0:T(8,128)(2,1)S(1)}, bf16[64,384]{1,0:T(8,128)(2,1)S(1)}, bf16[64,384]{1,0:T(8,128)(2,1)S(...) all-reduce(bf16[64,384]{1,0:T(8,128)(2,1)S(1)} %get-tuple-element.1, ...), channel_id=1, replica_groups=mesh['rep'=16,'fs'=4,'tp'=8] {'fs'}, use_global_device_ids=true, to_apply=%region_17.0 | all-reduce | flops 589824 | bytes 2359296 | tf_op jit(solution)/shard_map/psum | solution.py:38
  34.5 0.6 copy-done.20
  35.2 0.7 pad_maximum_fusion.1
  36.2 0.8 multiply_reduce_fusion.3
  37.3 0.8 copy-done.5
  40.7 69.0 %all-reduce.9 = (bf16[64,384]{0,1:T(8,128)(2,1)}, bf16[64,384]{0,1:T(8,128)(2,1)}, bf16[64,384]{0,1:T(8,128)(2,1)}, bf16[64,384]{0,1:T(8,128)(2,1)}, bf16[64,384...) all-reduce(bf16[64,384]{0,1:T(8,128)(2,1)S(1)} %get-tuple-element.1, ...), channel_id=1, replica_groups=mesh['rep'=16,'fs'=4,'tp'=8] {'rep'}, use_global_device_ids=true, to_apply=%region_25.0 | all-reduce | flops 590976 | bytes 2363904 | tf_op jit(solution)/shard_map/psum | solution.py:38
  109.8 0.9 constant_dynamic-update-slice_fusion.31
  110.7 0.8 constant_dynamic-update-slice_fusion.30
  111.5 0.8 constant_dynamic-update-slice_fusion.29
  112.3 0.8 constant_dynamic-update-slice_fusion.28
  113.1 0.8 constant_dynamic-update-slice_fusion.27
  113.9 0.8 constant_dynamic-update-slice_fusion.26
  114.7 0.8 constant_dynamic-update-slice_fusion.25
  115.5 1.0 multiply_reduce_fusion
  117.1 3.6 %all-to-all-start.1 = ((f32[4,1,384]{2,1,0:T(1,128)}), f32[4,1,384]{2,1,0:T(1,128)S(1)}, u32[]{:S(2)}, u32[]{:S(2)}) async-start(f32[4,1,384]{2,1,0:T(1,128)} %broadcast_in_dim.7), calls=%async_computation.1 | async-start | bytes 12288 | tf_op jit(solution)/shard_map/all_to_all | solution.py:112
  123.3 0.9 pad_maximum_fusion
  124.2 0.7 all-to-all-done.1
  124.8 23.3 %all-to-all-start = ((bf16[8,68,512]{2,1,0:T(8,128)(2,1)}), bf16[8,68,512]{2,1,0:T(8,128)(2,1)S(1)}, u32[]{:S(2)}, u32[]{:S(2)}) async-start(bf16[8,68,512]{2,1,0:T(8,128)(2,1)} %pad_maximum_fusion), calls=%async_computation | async-start | bytes 1179648 | tf_op jit(solution)/shard_map/all_to_all | solution.py:107
  148.1 1.1 copy.20
  149.2 1.1 copy.19
  150.2 0.7 maximum_convert_fusion
  152.2 6.0 %all-to-all-done = bf16[8,68,512]{2,1,0:T(8,128)(2,1)S(1)} async-done(((bf16[8,68,512]{2,1,0:T(8,128)(2,1)}), bf16[8,68,512]{2,1,0:T(8,128)(2,1)S(1)}, u32[]{:S(2)}, u32[]{:S(2)}) %all-to-all-start) | async-done | bytes 557088 | tf_op jit(solution)/shard_map/all_to_all | solution.py:107
  158.9 0.6 slice.340
  (111 shorter events, 10.4 us)
Async XLA Ops:
  0.6 2.4 %copy-start = (bf16[512,512]{1,0:T(8,128)(2,1)S(1)}, bf16[512,512]{1,0:T(8,128)(2,1)}, u32[]{:S(2)}) copy-start(bf16[512,512]{1,0:T(8,128)(2,1)} %param.6) | copy-start | bytes 1572868
  0.6 2.4 %copy-start.1 = (bf16[512,384]{1,0:T(8,128)(2,1)S(1)}, bf16[512,384]{1,0:T(8,128)(2,1)}, u32[]{:S(2)}) copy-start(bf16[512,384]{1,0:T(8,128)(2,1)} %param.7) | copy-start | bytes 1179652
  3.1 1.0 copy-start.3
  34.5 0.7 copy-start.20
  37.0 1.0 copy-start.5
  109.8 10.9 %copy-start.12 = (bf16[64,384]{0,1:T(8,128)(2,1)S(1)}, bf16[64,384]{0,1:T(8,128)(2,1)}, u32[]{:S(2)}) copy-start(bf16[64,384]{0,1:T(8,128)(2,1)} %get-tuple-element.38) | copy-start | bytes 147460
  109.8 10.9 %copy-start.13 = (bf16[64,384]{0,1:T(8,128)(2,1)S(1)}, bf16[64,384]{0,1:T(8,128)(2,1)}, u32[]{:S(2)}) copy-start(bf16[64,384]{0,1:T(8,128)(2,1)} %get-tuple-element.39) | copy-start | bytes 147460
  109.8 10.9 %copy-start.14 = (bf16[64,384]{0,1:T(8,128)(2,1)S(1)}, bf16[64,384]{0,1:T(8,128)(2,1)}, u32[]{:S(2)}) copy-start(bf16[64,384]{0,1:T(8,128)(2,1)} %get-tuple-element.40) | copy-start | bytes 147460
  109.8 10.9 %copy-start.15 = (bf16[64,384]{0,1:T(8,128)(2,1)S(1)}, bf16[64,384]{0,1:T(8,128)(2,1)}, u32[]{:S(2)}) copy-start(bf16[64,384]{0,1:T(8,128)(2,1)} %get-tuple-element.41) | copy-start | bytes 147460
  109.8 10.9 %copy-start.16 = (bf16[64,384]{0,1:T(8,128)(2,1)S(1)}, bf16[64,384]{0,1:T(8,128)(2,1)}, u32[]{:S(2)}) copy-start(bf16[64,384]{0,1:T(8,128)(2,1)} %get-tuple-element.42) | copy-start | bytes 147460
  109.8 10.9 %copy-start.17 = (bf16[64,384]{0,1:T(8,128)(2,1)S(1)}, bf16[64,384]{0,1:T(8,128)(2,1)}, u32[]{:S(2)}) copy-start(bf16[64,384]{0,1:T(8,128)(2,1)} %get-tuple-element.43) | copy-start | bytes 147460
  109.8 10.9 %copy-start.18 = (bf16[64,384]{0,1:T(8,128)(2,1)S(1)}, bf16[64,384]{0,1:T(8,128)(2,1)}, u32[]{:S(2)}) copy-start(bf16[64,384]{0,1:T(8,128)(2,1)} %get-tuple-element.44) | copy-start | bytes 147460
  109.8 10.9 %copy-start.19 = (bf16[64,384]{0,1:T(8,128)(2,1)S(1)}, bf16[64,384]{0,1:T(8,128)(2,1)}, u32[]{:S(2)}) copy-start(bf16[64,384]{0,1:T(8,128)(2,1)} %get-tuple-element.45) | copy-start | bytes 147460
  116.4 4.9 %copy-start.6 = (bf16[64,384]{0,1:T(8,128)(2,1)S(1)}, bf16[64,384]{0,1:T(8,128)(2,1)}, u32[]{:S(2)}) copy-start(bf16[64,384]{0,1:T(8,128)(2,1)} %get-tuple-element.48) | copy-start | bytes 147460
  116.4 4.9 %copy-start.7 = (bf16[64,384]{0,1:T(8,128)(2,1)S(1)}, bf16[64,384]{0,1:T(8,128)(2,1)}, u32[]{:S(2)}) copy-start(bf16[64,384]{0,1:T(8,128)(2,1)} %get-tuple-element.49) | copy-start | bytes 147460
  116.4 4.9 %copy-start.8 = (bf16[64,384]{0,1:T(8,128)(2,1)S(1)}, bf16[64,384]{0,1:T(8,128)(2,1)}, u32[]{:S(2)}) copy-start(bf16[64,384]{0,1:T(8,128)(2,1)} %get-tuple-element.50) | copy-start | bytes 147460
  116.4 4.9 %copy-start.9 = (bf16[64,384]{0,1:T(8,128)(2,1)S(1)}, bf16[64,384]{0,1:T(8,128)(2,1)}, u32[]{:S(2)}) copy-start(bf16[64,384]{0,1:T(8,128)(2,1)} %get-tuple-element.51) | copy-start | bytes 147460
  116.5 4.9 %copy-start.10 = (bf16[64,384]{0,1:T(8,128)(2,1)S(1)}, bf16[64,384]{0,1:T(8,128)(2,1)}, u32[]{:S(2)}) copy-start(bf16[64,384]{0,1:T(8,128)(2,1)} %get-tuple-element.52) | copy-start | bytes 147460
  116.5 4.9 %copy-start.11 = (bf16[64,384]{0,1:T(8,128)(2,1)S(1)}, bf16[64,384]{0,1:T(8,128)(2,1)}, u32[]{:S(2)}) copy-start(bf16[64,384]{0,1:T(8,128)(2,1)} %get-tuple-element.53) | copy-start | bytes 147460
  117.1 7.8 %all-to-all-start.1 = ((f32[4,1,384]{2,1,0:T(1,128)}), f32[4,1,384]{2,1,0:T(1,128)S(1)}, u32[]{:S(2)}, u32[]{:S(2)}) async-start(f32[4,1,384]{2,1,0:T(1,128)} %broadcast_in_dim.7), calls=%async_computation.1 | async-start | bytes 12288 | tf_op jit(solution)/shard_map/all_to_all | solution.py:112
  121.2 1.0 copy-start.2
  121.8 1.0 copy-start.4
  124.8 33.3 %all-to-all-start = ((bf16[8,68,512]{2,1,0:T(8,128)(2,1)}), bf16[8,68,512]{2,1,0:T(8,128)(2,1)S(1)}, u32[]{:S(2)}, u32[]{:S(2)}) async-start(bf16[8,68,512]{2,1,0:T(8,128)(2,1)} %pad_maximum_fusion), calls=%async_computation | async-start | bytes 1179648 | tf_op jit(solution)/shard_map/all_to_all | solution.py:107

commit v2 on v0

v2 whole, which is shorter than its diff:
```python
import jax
import jax.numpy as jnp
from jax import lax
from jax.experimental import pallas as pl
from jax.experimental.pallas import tpu as pltpu
from jax.sharding import PartitionSpec as P

KW = 3
ROWS = 64
UNITS = 48
PAD = 8
NORM_ROWS = 16
BF16 = jnp.bfloat16
F32 = jnp.float32


def contract(left, right, left_dim, right_dim):
    out = lax.dot_general(
        left, right, (((left_dim,), (right_dim,)), ((), ())), preferred_element_type=F32
    )
    return out.astype(BF16)


def pieces(array, rows):
    return [array[start : start + rows] for start in range(0, array.shape[0], rows)]


def call(kernel, out_shape, *args, scratch=()):
    whole = pl.BlockSpec(memory_space=pltpu.VMEM)
    return pl.pallas_call(
        kernel,
        out_shape=out_shape,
        in_specs=[whole] * len(args),
        out_specs=jax.tree.map(lambda _: whole, out_shape),
        scratch_shapes=list(scratch),
        compiler_params=pltpu.CompilerParams(vmem_limit_bytes=32 << 20),
    )(*args)


def corner(shape):
    row = lax.broadcasted_iota(jnp.int32, shape, 0)
    col = lax.broadcasted_iota(jnp.int32, shape, 1)
    return (row == 0) & (col == 0)


def pointwise_kernel(count, *refs):
    gate, up, act = refs[:count], refs[count : 2 * count], refs[2 * count : 3 * count]
    first, taps_in = refs[3 * count : 3 * count + 2]
    gate_grad, up_grad, hidden, taps_out, taps_first = refs[3 * count + 2 : 3 * count + 7]
    gate_pad, pre_pad = refs[3 * count + 7 :]
    width = taps_in.shape[1]
    taps = taps_in[...].astype(F32)
    tap = [taps[j : j + 1] for j in range(KW)]
    gate_pad[:PAD] = jnp.zeros((PAD, width), F32)
    for i in range(count):
        value = gate[i][...].astype(F32)
        if i == 0:
            value = jnp.where(corner(value.shape), first[0:1, 0:1].astype(F32), value)
        gate_pad[PAD + ROWS * i : PAD + ROWS * (i + 1)] = value
    sums = [jnp.zeros((1, width), F32) for _ in range(KW)]
    for i in range(count):
        base = PAD + ROWS * i - (KW - 1)
        shifted = [gate_pad[base + j : base + j + ROWS] for j in range(KW)]
        pre = tap[0] * shifted[0] + tap[1] * shifted[1] + tap[2] * shifted[2]
        sig = jax.nn.sigmoid(pre)
        silu = pre * sig
        up_value = up[i][...].astype(F32)
        act_value = act[i][...].astype(F32)
        rows = slice(ROWS * i, ROWS * (i + 1))
        hidden[rows] = (silu * up_value).astype(BF16)
        up_grad[rows] = (act_value * silu).astype(BF16)
        pre_grad = act_value * up_value * sig * (1.0 + pre * (1.0 - sig))
        pre_pad[rows] = pre_grad
        sums = [
            total + jnp.sum(value * pre_grad, axis=0, keepdims=True)
            for total, value in zip(sums, shifted)
        ]
    pre_pad[ROWS * count :] = jnp.zeros((PAD, width), F32)
    for i in range(count):
        base = ROWS * i
        later = [pre_pad[base + j : base + j + ROWS] for j in range(KW)]
        grad = tap[2] * later[0] + tap[1] * later[1] + tap[0] * later[2]
        gate_grad[base : base + ROWS] = grad.astype(BF16)
    taps_out[...] = jnp.concatenate(sums, axis=0).astype(BF16)
    taps_first[...] = sums[0][0:1, 0:1].astype(BF16)


def norms_kernel(count, *refs):
    gate, up, down = refs[:count], refs[count : 2 * count], refs[2 * count : 3 * count]
    part = refs[3 * count]
    packed, down_out = refs[3 * count + 1 :]
    slots, rows, width = part.shape
    packed[:, :rows] = part[...]
    split = []
    for group in (gate, up):
        total = jnp.zeros((1, width), F32)
        for ref in group:
            value = ref[...].astype(F32)
            total = total + jnp.sum(value * value, axis=0, keepdims=True)
        high = total.astype(BF16).astype(F32)
        split += [high, total - high]
    row = lax.broadcasted_iota(jnp.int32, (NORM_ROWS, width), 0)
    block = jnp.zeros((NORM_ROWS, width), F32)
    for i, value in enumerate(split):
        block = jnp.where(row == i, value, block)
    block = block.astype(BF16)
    for slot in range(slots):
        packed[slot, rows:] = block
    ones = jnp.ones((PAD, width), F32)
    square = jnp.concatenate([ref[...] for ref in down], axis=0).astype(F32)
    square = square * square
    down_out[...] = lax.dot_general(
        ones,
        square,
        (((1,), (1,)), ((), ())),
        precision=lax.Precision.HIGHEST,
        preferred_element_type=F32,
    )


def outputs_kernel(count, *refs):
    gate, up, down = refs[:count], refs[count : 2 * count], refs[2 * count : 3 * count]
    taps, first = refs[3 * count : 3 * count + 2]
    gate_out, up_out, down_out, taps_out = refs[3 * count + 2 :]
    for group, out in ((gate, gate_out), (up, up_out)):
        value = jnp.concatenate([ref[...] for ref in group], axis=0).astype(F32)
        out[...] = value.T
    for i, ref in enumerate(down):
        down_out[UNITS * i : UNITS * (i + 1)] = ref[...].astype(F32)
    value = taps[...].astype(F32)
    taps_out[...] = jnp.where(corner(value.shape), first[0:1, 0:1].astype(F32), value)


def reduce_kernel(got, in_grad, gate_rows, up_rows):
    slots, rows, _ = got.shape
    rows -= NORM_ROWS
    total = got[0].astype(F32)
    for slot in range(1, slots):
        total = total + got[slot].astype(F32)
    in_grad[...] = total[:rows].astype(BF16)
    gate_rows[...] = total[rows : rows + 1] + total[rows + 1 : rows + 2]
    up_rows[...] = total[rows + 2 : rows + 3] + total[rows + 3 : rows + 4]


def shards(inputs, w_gate, w_up, conv_taps, w_down, out_grad):
    tokens, width = inputs.shape
    units = w_gate.shape[1]
    n_tp = lax.axis_size("tp")
    shape = jax.ShapeDtypeStruct

    gate_part = contract(inputs, w_gate, 1, 0)
    up_part = contract(inputs, w_up, 1, 0)
    act_part = contract(out_grad, w_down, 1, 1)
    parts = [piece for part in (gate_part, up_part, act_part) for piece in pieces(part, ROWS)]
    parts = lax.psum((*parts, gate_part[:1, :1]), "fs")

    count = tokens // ROWS
    padded = pltpu.VMEM((tokens + PAD, units), F32)
    gate_grad, up_grad, hidden, taps_part, taps_first = call(
        lambda *refs: pointwise_kernel(count, *refs),
        (
            shape((tokens, units), BF16),
            shape((tokens, units), BF16),
            shape((tokens, units), BF16),
            shape((KW, units), BF16),
            shape((1, 1), BF16),
        ),
        *parts,
        conv_taps,
        scratch=(padded, padded),
    )
    grads = [
        contract(gate_grad, inputs, 0, 0),
        contract(up_grad, inputs, 0, 0),
        contract(hidden, out_grad, 0, 0),
    ]
    grads = [piece for grad in grads for piece in pieces(grad, UNITS)]
    *grads, taps_sum, taps_one = lax.psum((*grads, taps_part, taps_first), "rep")

    in_part = lax.dot_general(
        gate_grad, w_gate, (((1,), (1,)), ((), ())), preferred_element_type=F32
    ) + lax.dot_general(up_grad, w_up, (((1,), (1,)), ((), ())), preferred_element_type=F32)
    in_part = in_part.astype(BF16).reshape(n_tp, tokens // n_tp, width)

    count_units = units // UNITS
    packed, down_rows = call(
        lambda *refs: norms_kernel(count_units, *refs),
        (
            shape((n_tp, tokens // n_tp + NORM_ROWS, width), BF16),
            shape((PAD, units), F32),
        ),
        *grads,
        in_part,
    )
    got = lax.all_to_all(packed, "tp", 0, 0)
    down_rows = lax.psum(down_rows[0], "fs")
    grad_gate, grad_up, grad_down, grad_taps = call(
        lambda *refs: outputs_kernel(count_units, *refs),
        (
            shape((width, units), F32),
            shape((width, units), F32),
            shape((units, width), F32),
            shape((KW, units), F32),
        ),
        *grads,
        taps_sum,
        taps_one,
    )
    in_grad, gate_rows, up_rows = call(
        reduce_kernel,
        (
            shape((tokens // n_tp, width), BF16),
            shape((1, width), F32),
            shape((1, width), F32),
        ),
        got,
    )
    return (
        in_grad,
        grad_gate,
        grad_up,
        grad_down,
        grad_taps,
        gate_rows.reshape(width),
        up_rows.reshape(width),
        down_rows,
    )


def solution(mesh):
    return jax.shard_map(
        shards,
        mesh=mesh,
        in_specs=(
            P("rep", "fs"),
            P("fs", "tp"),
            P("fs", "tp"),
            P(None, "tp"),
            P("tp", "fs"),
            P("rep", "fs"),
        ),
        out_specs=(
            P(("rep", "tp"), "fs"),
            P("fs", "tp"),
            P("fs", "tp"),
            P("tp", "fs"),
            P(None, "tp"),
            P("fs"),
            P("fs"),
            P("tp"),
        ),
        check_vma=False,
    )
```

time: 274 us -> 145 us (0.53)
  waiting for transfers between devices: 180 us -> 1.63 us
  blocking collectives: 58.6 us -> 100 us
  starting transfers between devices: 0.12 us -> 23.5 us
  between operations: 13.9 us -> 0.76 us
  Pallas kernels: 0 us -> 7.52 us
  matrix products: 9.79 us -> 4.42 us
  other arithmetic: 2.95 us -> 0 us
    psum x2 -> x0, waiting for transfers between devices: 170 us -> none  [the longest x1 105 us: shards(): lax.psum(grad_gate.astype(jnp.bfloat16), 'rep').astype(jnp.float32)]
    psum x3, blocking collectives: 58.6 us -> 100 us  [the longest x1 63.6 us: shards(): lax.psum((*grads, taps_part, taps_first), 'rep')]
    all_to_all x0 -> x1, starting transfers between devices: none -> 23.5 us  [shards(): got = lax.all_to_all(packed, 'tp', 0, 0)]
    reduce_scatter x1 -> x0, waiting for transfers between devices: 9.19 us -> none  [shards(): lax.psum_scatter((contract(gate_rows, w_gate, 1, 1) + contract(up_rows, w...]
    pallas_call x0 -> x4, Pallas kernels: none -> 7.52 us  [call(): pl.pallas_call(kernel, out_shape=out_shape, in_specs=[whole] * len(args),...]
    dot_general x6, matrix products: 6.42 us -> 3.5 us  [contract(): lax.dot_general(left, right, (((left_dim,), (right_dim,)), ((), ())), pre...]
    unnamed x26 -> x14, local copies, waits for them, and re-layouts: 6.73 us -> 4.21 us
  transfers between devices with their start and end apart: 3 -> 1, of which waited for: 3 -> 1; matrix products, arithmetic and copies ran while one was open for 2% -> 0% of each run, Pallas kernels for 0% -> 2%
where the time goes in v2:
time: 145 us; the launch traced here: 144 us
  blocking collectives  100 us (69%)
  starting transfers between devices  23.5 us (16%)
  Pallas kernels  7.52 us (5%)
  local copies, waits for them, and re-layouts  6.23 us (4%)
  matrix products  4.42 us (3%)
  waiting for transfers between devices  1.63 us (1%)
    psum x1, blocking collectives, shards(): lax.psum((*grads, taps_part, taps_first), 'rep')  63.6 us
    psum x1, blocking collectives, shards(): parts = lax.psum((*parts, gate_part[:1, :1]), 'fs')  29.7 us
    all_to_all x1, starting transfers between devices, shards(): got = lax.all_to_all(packed, 'tp', 0, 0)  23.5 us
    pallas_call x4, Pallas kernels, call(): pl.pallas_call(kernel, out_shape=out_shape, in_specs=[whole] * len(args),...  7.52 us
    psum x1, blocking collectives, shards(): down_rows = lax.psum(down_rows[0], 'fs')  6.86 us
    unnamed x14, local copies, waits for them, and re-layouts  4.21 us
    dot_general x6, matrix products, contract(): lax.dot_general(left, right, (((left_dim,), (right_dim,)), ((), ())), pre...  3.5 us
  transfers between devices with their start and end apart: 1, of which 1 were waited for; matrix products, arithmetic and copies ran while one was open for 0% of the time, Pallas kernels for 2%

profile of v2, /device:TPU:1, one launch (start us, length us, event | category | flops | bytes accessed | tf_op | source)
XLA Modules:
  0.0 144.2 jit_solution(2798998031928144874)
XLA Ops:
  0.6 1.0 copy-done
  1.7 1.4 convolution_convert_fusion.5
  3.1 0.5 slice.224
  3.6 0.7 fusion.6
  4.3 0.4 copy-done.3
  4.7 0.4 convolution_convert_fusion.4
  5.2 0.6 copy-done.4
  5.9 0.5 convolution_convert_fusion.3
  6.4 29.7 %all-reduce.4 = (bf16[64,384]{1,0:T(8,128)(2,1)S(1)}, bf16[64,384]{1,0:T(8,128)(2,1)S(1)}, bf16[64,384]{1,0:T(8,128)(2,1)S(1)}, bf16[64,384]{1,0:T(8,128)(2,1)S(...) all-reduce(bf16[64,384]{1,0:T(8,128)(2,1)} %get-tuple-element.134, ...), channel_id=1, replica_groups=mesh['rep'=16,'fs'=4,'tp'=8] {'fs'}, use_global_device_ids=true, to_apply=%region_0.0 | all-reduce | flops 589825 | bytes 2359300 | tf_op jit(solution)/shard_map/psum | solution.py:155
  36.1 0.7 copy-done.1
  36.8 3.0 %shard_map.125 = (bf16[512,384]{1,0:T(8,128)(2,1)S(1)}, bf16[512,384]{1,0:T(8,128)(2,1)S(1)}, bf16[512,384]{1,0:T(8,128)(2,1)S(1)}, bf16[3,384]{1,0:T(4,128)(2,1)S(1)}, bf16[1,1]{1,0:T(2,128)(2,1)}) custom-call(bf16[64,384]{1,0:T(8,128)(2,1)S(1)} %get-tuple-element.62.refs_0_, bf16[64,384]{1,0:T(8,128)(2,1)S(1)} %get-tuple-element.63.refs_1_, ...), custom_call_target="tpu_custom_call" | custom-call | tf_op jit(solution)/shard_map/pallas_call | solution.py:30
  40.2 0.6 copy-done.2
  40.8 0.5 fusion.7
  41.8 0.4 convolution_convert_fusion.1
  42.2 0.7 fusion.2
  42.8 0.5 fusion
  43.3 0.8 copy-done.6
  44.1 63.6 %all-reduce.5 = (bf16[48,512]{1,0:T(8,128)(2,1)S(1)}, bf16[48,512]{1,0:T(8,128)(2,1)S(1)}, bf16[48,512]{1,0:T(8,128)(2,1)S(1)}, bf16[48,512]{1,0:T(8,128)(2,1)S(...) all-reduce(bf16[48,512]{1,0:T(8,128)(2,1)S(1)} %get-tuple-element.1, ...), channel_id=1, replica_groups=mesh['rep'=16,'fs'=4,'tp'=8] {'rep'}, use_global_device_ids=true, to_apply=%region_25.0 | all-reduce | flops 590977 | bytes 2363908 | tf_op jit(solution)/shard_map/psum | solution.py:178
  107.7 1.6 %shard_map.126 = (bf16[8,80,512]{2,1,0:T(8,128)(2,1)}, f32[8,384]{1,0:T(8,128)S(1)}) custom-call(bf16[48,512]{1,0:T(8,128)(2,1)S(1)} %get-tuple-element.36.refs_0_, bf16[48,512]{1,0:T(8,128)(2,1)S(1)} %get-tuple-element.37.refs_1_, bf16[48,512]{1,0:T(8,128)(2,1)S(1)} %get-tuple-element.38.refs_2_, bf16[48,512]{1,0:T(8,128)(2,1)S(1)} %get-tuple-element.39.refs_3_, ...), custom_call_target="tpu_custom_call" | custom-call | tf_op jit(solution)/shard_map/pallas_call | solution.py:30
  109.3 23.5 %all-to-all-start = ((bf16[8,80,512]{2,1,0:T(8,128)(2,1)}), bf16[8,80,512]{2,1,0:T(8,128)(2,1)S(1)}, u32[]{:S(2)}, u32[]{:S(2)}) async-start(bf16[8,80,512]{2,1,0:T(8,128)(2,1)} %get-tuple-element.25), calls=%async_computation | async-start | bytes 1310720 | tf_op jit(solution)/shard_map/all_to_all | solution.py:195
  132.8 2.2 %shard_map.128 = (f32[512,384]{1,0:T(8,128)}, f32[512,384]{1,0:T(8,128)}, f32[384,512]{1,0:T(8,128)}, f32[3,384]{1,0:T(4,128)}) custom-call(bf16[48,512]{1,0:T(8,128)(2,1)S(1)} %get-tuple-element.36.refs_0_, bf16[48,512]{1,0:T(8,128)(2,1)S(1)} %get-tuple-element.37.refs_1_, bf16[48,512]{1,0:T(8,128)(2,1)S(1)} %get-tuple-element.38.refs_2_, ...), custom_call_target="tpu_custom_call" | custom-call | tf_op jit(solution)/shard_map/pallas_call | solution.py:30
  135.0 6.9 %psum.415 = f32[384]{0:T(512)} all-reduce(f32[384]{0:T(512)S(1)} %slice_reduce_fusion), channel_id=1, replica_groups=mesh['rep'=16,'fs'=4,'tp'=8] {'fs'}, use_global_device_ids=true, to_apply=%region_51.0 | all-reduce | flops 384 | bytes 3072 | tf_op jit(solution)/shard_map/psum | solution.py:196
  141.9 1.6 %all-to-all-done.got = bf16[8,80,512]{2,1,0:T(8,128)(2,1)S(1)} async-done(((bf16[8,80,512]{2,1,0:T(8,128)(2,1)}), bf16[8,80,512]{2,1,0:T(8,128)(2,1)S(1)}, u32[]{:S(2)}, u32[]{:S(2)}) %all-to-all-start) | async-done | bytes 655392 | tf_op jit(solution)/shard_map/all_to_all | solution.py:195
  143.5 0.7 shard_map.127
  (14 shorter events, 1.1 us)
Async XLA Ops:
  0.6 1.0 copy-start
  3.6 1.1 copy-start.3
  4.7 1.0 copy-start.4
  4.7 1.2 copy-start.5
  36.1 0.7 copy-start.1
  39.8 1.0 copy-start.2
  43.3 0.8 copy-start.6
  109.3 34.2 %all-to-all-start = ((bf16[8,80,512]{2,1,0:T(8,128)(2,1)}), bf16[8,80,512]{2,1,0:T(8,128)(2,1)S(1)}, u32[]{:S(2)}, u32[]{:S(2)}) async-start(bf16[8,80,512]{2,1,0:T(8,128)(2,1)} %get-tuple-element.25), calls=%async_computation | async-start | bytes 1310720 | tf_op jit(solution)/shard_map/all_to_all | solution.py:195

commit v3 on v2

--- a/solution.py
+++ b/solution.py
@@ -9,80 +9,135 @@
 ROWS = 64
 UNITS = 48
 PAD = 8
+LANES = 128
+STRIP = 32
 NORM_ROWS = 16
 BF16 = jnp.bfloat16
 F32 = jnp.float32
 
 
-def contract(left, right, left_dim, right_dim):
-    out = lax.dot_general(
-        left, right, (((left_dim,), (right_dim,)), ((), ())), preferred_element_type=F32
-    )
-    return out.astype(BF16)
-
-
-def pieces(array, rows):
-    return [array[start : start + rows] for start in range(0, array.shape[0], rows)]
-
-
-def call(kernel, out_shape, *args, scratch=()):
+def call(kernel, out_shape, *args, far=(), scratch=()):
     whole = pl.BlockSpec(memory_space=pltpu.VMEM)
+    scratch = [*scratch]
+    if far:
+        scratch += [pltpu.VMEM(array.shape, array.dtype) for array in far]
+        scratch += [pltpu.SemaphoreType.DMA((len(far),))]
+    args = (*args, *[pltpu.with_memory_space_constraint(array, pltpu.HBM) for array in far])
     return pl.pallas_call(
         kernel,
         out_shape=out_shape,
-        in_specs=[whole] * len(args),
+        in_specs=[whole] * (len(args) - len(far))
+        + [pl.BlockSpec(memory_space=pltpu.HBM)] * len(far),
         out_specs=jax.tree.map(lambda _: whole, out_shape),
         scratch_shapes=list(scratch),
         compiler_params=pltpu.CompilerParams(vmem_limit_bytes=32 << 20),
     )(*args)
 
 
+def fetch(sources, targets, sems):
+    copies = [
+        pltpu.make_async_copy(source, target, sems.at[k])
+        for k, (source, target) in enumerate(zip(sources, targets))
+    ]
+    for copy in copies:
+        copy.start()
+    return copies
+
+
 def corner(shape):
     row = lax.broadcasted_iota(jnp.int32, shape, 0)
     col = lax.broadcasted_iota(jnp.int32, shape, 1)
     return (row == 0) & (col == 0)
 
 
-def pointwise_kernel(count, *refs):
+def matmul(left, right, left_dim, right_dim):
+    return lax.dot_general(
+        left, right, (((left_dim,), (right_dim,)), ((), ())), preferred_element_type=F32
+    )
+
+
+def forward_kernel(*refs):
+    sources, outs, first = refs[:5], refs[5:-7], refs[-7]
+    local, sems = refs[-6:-1], refs[-1]
+    count = len(outs) // 3
+    inputs, w_gate, w_up, out_grad, w_down = local
+    copies = fetch(sources, local, sems)
+    for k, ref in enumerate((w_gate, w_up, w_down)):
+        copies[k + 1].wait()
+        if k == 0:
+            copies[0].wait()
+        if k == 2:
+            copies[4].wait()
+            value = matmul(out_grad[...], w_down[...], 1, 1)
+        else:
+            value = matmul(inputs[...], ref[...], 1, 0)
+        for i in range(count):
+            outs[k * count + i][...] = value[ROWS * i : ROWS * (i + 1)].astype(BF16)
+        if k == 0:
+            first[...] = value[0:1, 0:1].astype(BF16)
+
+
+def backward_kernel(count, *refs):
     gate, up, act = refs[:count], refs[count : 2 * count], refs[2 * count : 3 * count]
-    first, taps_in = refs[3 * count : 3 * count + 2]
-    gate_grad, up_grad, hidden, taps_out, taps_first = refs[3 * count + 2 : 3 * count + 7]
-    gate_pad, pre_pad = refs[3 * count + 7 :]
+    first = refs[3 * count]
+    sources = refs[3 * count + 1 : 3 * count + 6]
+    gate_pad, pre_pad, gate_grad, up_grad, hidden = refs[-11:-6]
+    local, sems = refs[-6:-1], refs[-1]
+    taps_in, inputs, out_grad, w_gate, w_up = local
+    *grads, taps_out, taps_first, part = refs[3 * count + 6 : -11]
+    copies = fetch(sources, local, sems)
+    copies[0].wait()
     width = taps_in.shape[1]
     taps = taps_in[...].astype(F32)
-    tap = [taps[j : j + 1] for j in range(KW)]
+    tokens = ROWS * count
     gate_pad[:PAD] = jnp.zeros((PAD, width), F32)
+    pre_pad[tokens:] = jnp.zeros((PAD, width), F32)
     for i in range(count):
-        value = gate[i][...].astype(F32)
-        if i == 0:
-            value = jnp.where(corner(value.shape), first[0:1, 0:1].astype(F32), value)
-        gate_pad[PAD + ROWS * i : PAD + ROWS * (i + 1)] = value
-    sums = [jnp.zeros((1, width), F32) for _ in range(KW)]
-    for i in range(count):
-        base = PAD + ROWS * i - (KW - 1)
-        shifted = [gate_pad[base + j : base + j + ROWS] for j in range(KW)]
-        pre = tap[0] * shifted[0] + tap[1] * shifted[1] + tap[2] * shifted[2]
-        sig = jax.nn.sigmoid(pre)
-        silu = pre * sig
-        up_value = up[i][...].astype(F32)
-        act_value = act[i][...].astype(F32)
-        rows = slice(ROWS * i, ROWS * (i + 1))
-        hidden[rows] = (silu * up_value).astype(BF16)
-        up_grad[rows] = (act_value * silu).astype(BF16)
-        pre_grad = act_value * up_value * sig * (1.0 + pre * (1.0 - sig))
-        pre_pad[rows] = pre_grad
-        sums = [
-            total + jnp.sum(value * pre_grad, axis=0, keepdims=True)
-            for total, value in zip(sums, shifted)
-        ]
-    pre_pad[ROWS * count :] = jnp.zeros((PAD, width), F32)
-    for i in range(count):
-        base = ROWS * i
-        later = [pre_pad[base + j : base + j + ROWS] for j in range(KW)]
-        grad = tap[2] * later[0] + tap[1] * later[1] + tap[0] * later[2]
-        gate_grad[base : base + ROWS] = grad.astype(BF16)
-    taps_out[...] = jnp.concatenate(sums, axis=0).astype(BF16)
-    taps_first[...] = sums[0][0:1, 0:1].astype(BF16)
+        gate_pad[PAD + ROWS * i : PAD + ROWS * (i + 1)] = gate[i][...].astype(F32)
+    head = gate_pad[PAD : 2 * PAD, :LANES]
+    gate_pad[PAD : 2 * PAD, :LANES] = jnp.where(
+        corner(head.shape), first[0:1, 0:1].astype(F32), head
+    )
+    for lane in range(0, width, LANES):
+        cols = slice(lane, lane + LANES)
+        tap = [jnp.broadcast_to(taps[j : j + 1, cols], (STRIP, LANES)) for j in range(KW)]
+        sums = [jnp.zeros((STRIP, LANES), F32) for _ in range(KW)]
+        for start in range(0, tokens, STRIP):
+            i, inner = divmod(start, ROWS)
+            base = PAD + start - (KW - 1)
+            shifted = [gate_pad[base + j : base + j + STRIP, cols] for j in range(KW)]
+            pre = tap[0] * shifted[0] + tap[1] * shifted[1] + tap[2] * shifted[2]
+            sig = jax.nn.sigmoid(pre)
+            silu = pre * sig
+            up_value = up[i][inner : inner + STRIP, cols].astype(F32)
+            act_value = act[i][inner : inner + STRIP, cols].astype(F32)
+            rows = slice(start, start + STRIP)
+            hidden[rows, cols] = (silu * up_value).astype(BF16)
+            up_grad[rows, cols] = (act_value * silu).astype(BF16)
+            pre_grad = act_value * up_value * sig * (1.0 + pre * (1.0 - sig))
+            pre_pad[rows, cols] = pre_grad
+            sums = [total + value * pre_grad for total, value in zip(sums, shifted)]
+        for start in range(0, tokens, STRIP):
+            later = [pre_pad[start + j : start + j + STRIP, cols] for j in range(KW)]
+            grad = tap[2] * later[0] + tap[1] * later[1] + tap[0] * later[2]
+            gate_grad[start : start + STRIP, cols] = grad.astype(BF16)
+        for j in range(KW):
+            row = jnp.sum(sums[j], axis=0, keepdims=True)
+            taps_out[j : j + 1, cols] = row.astype(BF16)
+            if lane == 0 and j == 0:
+                taps_first[...] = row[0:1, 0:1].astype(BF16)
+    for copy in copies[1:]:
+        copy.wait()
+    x = inputs[...]
+    for k, (left, right) in enumerate(((gate_grad, x), (up_grad, x), (hidden, out_grad[...]))):
+        value = matmul(left[...], right, 0, 0)
+        for i in range(width // UNITS):
+            piece = value[UNITS * i : UNITS * (i + 1)].astype(BF16)
+            grads[k * (width // UNITS) + i][...] = piece
+    value = matmul(gate_grad[...], w_gate[...], 1, 1) + matmul(up_grad[...], w_up[...], 1, 1)
+    slots, rows, _ = part.shape
+    for slot in range(slots):
+        part[slot] = value[rows * slot : rows * (slot + 1)].astype(BF16)
 
 
 def norms_kernel(count, *refs):
@@ -148,41 +203,31 @@
     n_tp = lax.axis_size("tp")
     shape = jax.ShapeDtypeStruct
 
-    gate_part = contract(inputs, w_gate, 1, 0)
-    up_part = contract(inputs, w_up, 1, 0)
-    act_part = contract(out_grad, w_down, 1, 1)
-    parts = [piece for part in (gate_part, up_part, act_part) for piece in pieces(part, ROWS)]
-    parts = lax.psum((*parts, gate_part[:1, :1]), "fs")
-
     count = tokens // ROWS
+    count_units = units // UNITS
+    one = shape((1, 1), BF16)
+    parts = call(
+        forward_kernel,
+        (*[shape((ROWS, units), BF16)] * (3 * count), one),
+        far=(inputs, w_gate, w_up, out_grad, w_down),
+    )
+    parts = lax.psum(tuple(parts), "fs")
     padded = pltpu.VMEM((tokens + PAD, units), F32)
-    gate_grad, up_grad, hidden, taps_part, taps_first = call(
-        lambda *refs: pointwise_kernel(count, *refs),
-        (
-            shape((tokens, units), BF16),
-            shape((tokens, units), BF16),
-            shape((tokens, units), BF16),
+    rounded = pltpu.VMEM((tokens, units), BF16)
+    *grads, in_part = call(
+        lambda *refs: backward_kernel(count, *refs),
+        (
+            *[shape((UNITS, width), BF16)] * (3 * count_units),
             shape((KW, units), BF16),
-            shape((1, 1), BF16),
+            one,
+            shape((n_tp, tokens // n_tp, width), BF16),
         ),
         *parts,
-        conv_taps,
-        scratch=(padded, padded),
-    )
-    grads = [
-        contract(gate_grad, inputs, 0, 0),
-        contract(up_grad, inputs, 0, 0),
-        contract(hidden, out_grad, 0, 0),
-    ]
-    grads = [piece for grad in grads for piece in pieces(grad, UNITS)]
-    *grads, taps_sum, taps_one = lax.psum((*grads, taps_part, taps_first), "rep")
-
-    in_part = lax.dot_general(
-        gate_grad, w_gate, (((1,), (1,)), ((), ())), preferred_element_type=F32
-    ) + lax.dot_general(up_grad, w_up, (((1,), (1,)), ((), ())), preferred_element_type=F32)
-    in_part = in_part.astype(BF16).reshape(n_tp, tokens // n_tp, width)
-
-    count_units = units // UNITS
+        far=(conv_taps, inputs, out_grad, w_gate, w_up),
+        scratch=(padded, padded, rounded, rounded, rounded),
+    )
+    *grads, taps_sum, taps_one = lax.psum(tuple(grads), "rep")
+
     packed, down_rows = call(
         lambda *refs: norms_kernel(count_units, *refs),
         (

time: 145 us -> 138 us (0.952)
  local copies, waits for them, and re-layouts: 6.23 us -> 0.02 us
  matrix products: 4.42 us -> 0 us
  Pallas kernels: 7.52 us -> 11.7 us
    dot_general x8 -> x0, matrix products: 4.42 us -> none  [the longest x6 3.5 us: contract(): lax.dot_general(left, right, (((left_dim,), (right_dim,)), ((), ())), pre...]
    unnamed x14 -> x0, local copies, waits for them, and re-layouts: 4.21 us -> none
    pallas_call x4 -> x5, Pallas kernels: 7.52 us -> 11.7 us  [call(): pl.pallas_call(kernel, out_shape=out_shape, in_specs=[whole] * (len(args)...]
    slice x6 -> x0, local copies, waits for them, and re-layouts: 2 us -> none  [the longest x5 1.48 us: pieces(): array[start:start + rows]]
where the time goes in v3:
time: 138 us
  blocking collectives  100 us (72%)
  starting transfers between devices  23.5 us (17%)
  Pallas kernels  11.7 us (8%)
  waiting for transfers between devices  1.63 us (1%)
    psum x1, blocking collectives, shards(): *grads, taps_sum, taps_one = lax.psum(tuple(grads), 'rep')  63.7 us
    psum x1, blocking collectives, shards(): parts = lax.psum(tuple(parts), 'fs')  29.7 us
    all_to_all x1, starting transfers between devices, shards(): got = lax.all_to_all(packed, 'tp', 0, 0)  23.5 us
    pallas_call x5, Pallas kernels, call(): pl.pallas_call(kernel, out_shape=out_shape, in_specs=[whole] * (len(args)...  11.7 us
    psum x1, blocking collectives, shards(): down_rows = lax.psum(down_rows[0], 'fs')  6.86 us
  transfers between devices with their start and end apart: 1, of which 1 were waited for; matrix products, arithmetic and copies ran while one was open for 0% of the time, Pallas kernels for 2%

profile of v3, /device:TPU:1, one launch (start us, length us, event | category | flops | bytes accessed | tf_op | source)
XLA Modules:
  0.0 137.7 jit_solution(10281323351370313648)
XLA Ops:
  0.6 2.7 %shard_map.125 = (bf16[64,384]{1,0:T(8,128)(2,1)S(1)}, bf16[64,384]{1,0:T(8,128)(2,1)S(1)}, bf16[64,384]{1,0:T(8,128)(2,1)S(1)}, bf16[64,384]{1,0:T(8,128)(2,1)S...) custom-call(bf16[512,512]{1,0:T(8,128)(2,1)} %refs_26_.1, ...), custom_call_target="tpu_custom_call" | custom-call | tf_op jit(solution)/shard_map/pallas_call | solution.py:26
  3.3 29.7 %all-reduce.4 = (bf16[64,384]{1,0:T(8,128)(2,1)S(1)}, bf16[64,384]{1,0:T(8,128)(2,1)S(1)}, bf16[64,384]{1,0:T(8,128)(2,1)S(1)}, bf16[64,384]{1,0:T(8,128)(2,1)S(...) all-reduce(bf16[64,384]{1,0:T(8,128)(2,1)S(1)} %get-tuple-element.6, ...), channel_id=1, replica_groups=mesh['rep'=16,'fs'=4,'tp'=8] {'fs'}, use_global_device_ids=true, to_apply=%region_0.0 | all-reduce | flops 589825 | bytes 2359300 | tf_op jit(solution)/shard_map/psum | solution.py:214
  33.0 4.6 %shard_map.126 = (bf16[48,512]{1,0:T(8,128)(2,1)S(1)}, bf16[48,512]{1,0:T(8,128)(2,1)S(1)}, bf16[48,512]{1,0:T(8,128)(2,1)S(1)}, bf16[48,512]{1,0:T(8,128)(2,1)S...) custom-call(bf16[64,384]{1,0:T(8,128)(2,1)S(1)} %get-tuple-element.1, ...), custom_call_target="tpu_custom_call" | custom-call | tf_op jit(solution)/shard_map/pallas_call | solution.py:26
  37.6 63.7 %all-reduce.5 = (bf16[48,512]{1,0:T(8,128)(2,1)S(1)}, bf16[48,512]{1,0:T(8,128)(2,1)S(1)}, bf16[48,512]{1,0:T(8,128)(2,1)S(1)}, bf16[48,512]{1,0:T(8,128)(2,1)S(...) all-reduce(bf16[48,512]{1,0:T(8,128)(2,1)S(1)} %get-tuple-element.9, ...), channel_id=1, replica_groups=mesh['rep'=16,'fs'=4,'tp'=8] {'rep'}, use_global_device_ids=true, to_apply=%region_25.0 | all-reduce | flops 590977 | bytes 2363908 | tf_op jit(solution)/shard_map/psum | solution.py:229
  101.2 1.5 %shard_map.127 = (bf16[8,80,512]{2,1,0:T(8,128)(2,1)}, f32[8,384]{1,0:T(8,128)S(1)}) custom-call(bf16[48,512]{1,0:T(8,128)(2,1)S(1)} %get-tuple-element.130.refs_0_, bf16[48,512]{1,0:T(8,128)(2,1)S(1)} %get-tuple-element.131.refs_1_, bf16[48,512]{1,0:T(8,128)(2,1)S(1)} %get-tuple-element.132.refs_2_, bf16[48,512]{1,0:T(8,128)(2,1)S(1)} %get-tuple-element.133.refs_3_, ...), custom_call_target="tpu_custom_call" | custom-call | tf_op jit(solution)/shard_map/pallas_call | solution.py:26
  102.8 23.5 %all-to-all-start = ((bf16[8,80,512]{2,1,0:T(8,128)(2,1)}), bf16[8,80,512]{2,1,0:T(8,128)(2,1)S(1)}, u32[]{:S(2)}, u32[]{:S(2)}) async-start(bf16[8,80,512]{2,1,0:T(8,128)(2,1)} %get-tuple-element.119), calls=%async_computation | async-start | bytes 1310720 | tf_op jit(solution)/shard_map/all_to_all | solution.py:240
  126.3 2.2 %shard_map.129 = (f32[512,384]{1,0:T(8,128)}, f32[512,384]{1,0:T(8,128)}, f32[384,512]{1,0:T(8,128)}, f32[3,384]{1,0:T(4,128)}) custom-call(bf16[48,512]{1,0:T(8,128)(2,1)S(1)} %get-tuple-element.130.refs_0_, bf16[48,512]{1,0:T(8,128)(2,1)S(1)} %get-tuple-element.131.refs_1_, bf16[48,512]{1,0:T(8,128)(2,1)S(1)} %get-tuple-element.132.refs_2_, ...), custom_call_target="tpu_custom_call" | custom-call | tf_op jit(solution)/shard_map/pallas_call | solution.py:26
  128.5 6.9 %psum.415 = f32[384]{0:T(512)} all-reduce(f32[384]{0:T(512)S(1)} %slice_reduce_fusion), channel_id=1, replica_groups=mesh['rep'=16,'fs'=4,'tp'=8] {'fs'}, use_global_device_ids=true, to_apply=%region_51.0 | all-reduce | flops 384 | bytes 3072 | tf_op jit(solution)/shard_map/psum | solution.py:241
  135.4 1.6 %all-to-all-done.got = bf16[8,80,512]{2,1,0:T(8,128)(2,1)S(1)} async-done(((bf16[8,80,512]{2,1,0:T(8,128)(2,1)}), bf16[8,80,512]{2,1,0:T(8,128)(2,1)S(1)}, u32[]{:S(2)}, u32[]{:S(2)}) %all-to-all-start) | async-done | bytes 655392 | tf_op jit(solution)/shard_map/all_to_all | solution.py:240
  137.0 0.7 shard_map.128
  (1 shorter events, 0.0 us)
Async XLA Ops:
  102.8 34.2 %all-to-all-start = ((bf16[8,80,512]{2,1,0:T(8,128)(2,1)}), bf16[8,80,512]{2,1,0:T(8,128)(2,1)S(1)}, u32[]{:S(2)}, u32[]{:S(2)}) async-start(bf16[8,80,512]{2,1,0:T(8,128)(2,1)} %get-tuple-element.119), calls=%async_computation | async-start | bytes 1310720 | tf_op jit(solution)/shard_map/all_to_all | solution.py:240
